TPU v7x, 32 devices: a whole 2x2x4 slice. The times are simulated.
32 devices in a mesh: ep: 8 (over z, x), tp: 4 (over y, core).
Axes of the slice: x: 2, y: 2, z: 4, core: 2. Of those that a mesh axis runs over, the one named last changes fastest.
Arguments:
- query_rows: bfloat16 [3072, 1024], P('ep', 'tp'), may hold values from -8 to 8
- key_rows: bfloat16 [3072, 256], P('ep'), may hold values from -8 to 8
- value_rows: bfloat16 [3072, 256], P('ep'), may hold values from -6 to 6
- query_gain: float32 [64], replicated, may hold values from 0.3 to 6
- key_gain: float32 [64], replicated, may hold values from 0.3 to 6
- out_weight: bfloat16 [1024, 2048], P('tp'), may hold values from -0.1875 to 0.1875
- mixer_gain: float32 [2048], replicated, may hold values from 0.1 to 1.9
- expert_input: bfloat16 [2048, 2048], P('ep'), may hold values from -6 to 6
- expert_ids: int32 [2048, 2], P('ep'), may hold values from 0 to 7, all different within a row; in each aligned block of 256 rows (0 to 255, 256 to 511, ...) at most 96 rows name the same one
- gate_score: float32 [2048, 2], P('ep'), may hold values from 0.05 to 1
- expert_gain: float32 [2048], replicated, may hold values from 0.1 to 1.9
- gate_weight: bfloat16 [8, 2048, 4096], P('ep', None, 'tp'), may hold values from -0.125 to 0.125
- up_weight: bfloat16 [8, 2048, 4096], P('ep', None, 'tp'), may hold values from -0.125 to 0.125
- down_weight: bfloat16 [8, 4096, 2048], P('ep', 'tp'), may hold values from -0.09375 to 0.09375
- shared_gate: bfloat16 [2048, 2048], P(None, 'tp'), may hold values from -0.125 to 0.125
- shared_up: bfloat16 [2048, 2048], P(None, 'tp'), may hold values from -0.125 to 0.125
- shared_down: bfloat16 [2048, 2048], P('tp'), may hold values from -0.125 to 0.125
Outputs:
- mixer_out: bfloat16 [3072, 2048], P('ep')
- expert_out: bfloat16 [2048, 2048], P('ep', 'tp')
Inputs may be any that keep to these rules, and one draw needn't show every extreme that they name: `expert_ids`: each row names 2 different experts. In each aligned block of 256 rows (the rows of one device) no expert is named by more than 96 rows, a bound that some block reaches.
All inputs are finite; a program needn't handle non-finite values.
Results may differ from a plain program's by a relative error of at most 0.02.
The roundings to bfloat16 on the way count: a program that leaves them out, or rounds other values in their place, can miss the bound.
Values may be sent and summed in bfloat16 or wider, within the bound.
A program may use at most 128 MiB of HBM per device.

v0:
```python
import math
import jax
import jax.numpy as jnp
from jax import lax
from jax.sharding import PartitionSpec as P

HEADS = 16
KV_HEADS = 4
HEAD_DIM = 64
GRID_W = 64
EPSILON = 1e-06
ROUTED_SCALE = 2.5


def rotary_angles(position):
    grid_row = (position // GRID_W).astype(jnp.float32)
    grid_col = (position % GRID_W).astype(jnp.float32)
    quarter = HEAD_DIM // 4
    inverse = 10000.0 ** (-jnp.arange(quarter, dtype=jnp.float32) / quarter)
    return jnp.concatenate([grid_row[:, None] * inverse, grid_col[:, None] * inverse], axis=1)


def normalize_rotate(heads_in, gain_vector, angles):
    widened = heads_in.astype(jnp.float32)
    scaled = widened * lax.rsqrt(jnp.mean(widened * widened, axis=-1, keepdims=True) + EPSILON)
    scaled = scaled * gain_vector
    half_dim = scaled.shape[-1] // 2
    front_half = scaled[..., :half_dim]
    back_half = scaled[..., half_dim:]
    cosine_table = jnp.cos(angles)[:, None, :]
    sine_table = jnp.sin(angles)[:, None, :]
    turned = jnp.concatenate(
        [
            front_half * cosine_table - back_half * sine_table,
            front_half * sine_table + back_half * cosine_table,
        ],
        axis=-1,
    )
    return turned.astype(jnp.bfloat16)


def mixer_half(query_rows, key_rows, value_rows, query_gain, key_gain, out_weight, mixer_gain):
    local_rows = query_rows.shape[0]
    lane_heads = query_rows.shape[1] // HEAD_DIM
    group = HEADS // KV_HEADS
    lane_kv = max(1, lane_heads // group)
    local_group = lane_heads // lane_kv
    first_kv = lax.axis_index("tp") * lane_heads // group
    offset = lax.axis_index("ep") * local_rows
    angles = rotary_angles(offset + jnp.arange(local_rows, dtype=jnp.int32))
    query_rot = normalize_rotate(
        query_rows.reshape(local_rows, lane_heads, HEAD_DIM), query_gain, angles
    )
    query_grouped = query_rot.reshape(local_rows, lane_kv, local_group, HEAD_DIM)
    key_cols = lax.dynamic_slice_in_dim(key_rows, first_kv * HEAD_DIM, lane_kv * HEAD_DIM, 1)
    value_cols = lax.dynamic_slice_in_dim(value_rows, first_kv * HEAD_DIM, lane_kv * HEAD_DIM, 1)
    key_rot = normalize_rotate(key_cols.reshape(local_rows, lane_kv, HEAD_DIM), key_gain, angles)
    stacked = jnp.concatenate([key_rot.reshape(local_rows, lane_kv * HEAD_DIM), value_cols], axis=1)
    scale_factor = HEAD_DIM ** (-0.5)
    key_width = lane_kv * HEAD_DIM

    def step_block(state, block_rows):
        row_peak, row_total, accum = state
        block_keys = block_rows[:, :key_width].reshape(block_rows.shape[0], lane_kv, HEAD_DIM)
        block_values = block_rows[:, key_width:].reshape(block_rows.shape[0], lane_kv, HEAD_DIM)
        scores = (
            jnp.einsum(
                "qkgd,skd->kgqs", query_grouped, block_keys, preferred_element_type=jnp.float32
            )
            * scale_factor
        )
        new_peak = jnp.maximum(row_peak, jnp.max(scores, axis=3))
        shrink = jnp.exp(row_peak - new_peak)
        exponent = jnp.exp(scores - new_peak[..., None])
        row_total = row_total * shrink + jnp.sum(exponent, axis=3)
        accum = accum * shrink[..., None] + jnp.einsum(
            "kgqs,skd->kgqd",
            exponent.astype(jnp.bfloat16),
            block_values,
            preferred_element_type=jnp.float32,
        )
        return ((new_peak, row_total, accum), None)

    start_state = (
        jnp.full((lane_kv, local_group, local_rows), -jnp.inf, jnp.float32),
        jnp.zeros((lane_kv, local_group, local_rows), jnp.float32),
        jnp.zeros((lane_kv, local_group, local_rows, HEAD_DIM), jnp.float32),
    )
    carry = start_state
    piece = lax.all_gather(stacked, "ep", axis=0, tiled=True)
    shard_count = piece.shape[0] // local_rows
    per_block = math.gcd(shard_count, max(1, 2048 // local_rows))
    block_rows = per_block * local_rows
    blocks = piece.reshape(piece.shape[0] // block_rows, block_rows, piece.shape[1])
    carry, unused = lax.scan(step_block, carry, blocks)
    row_peak, row_total, accum = carry
    attended = (accum / row_total[..., None]).astype(jnp.bfloat16)
    lane_weight = out_weight.reshape(lane_kv, local_group, HEAD_DIM, out_weight.shape[1])
    partial_value = jnp.einsum(
        "kgqd,kgde->qe", attended, lane_weight, preferred_element_type=jnp.float32
    )
    mixer_sum = lax.psum(partial_value.astype(jnp.bfloat16), "tp").astype(jnp.float32)
    mixer_scale = lax.rsqrt(jnp.mean(mixer_sum * mixer_sum, axis=1, keepdims=True) + EPSILON)
    return (mixer_sum * mixer_scale * mixer_gain).astype(jnp.bfloat16)


def expert_half(
    expert_input,
    expert_ids,
    gate_score,
    expert_gain,
    gate_weight,
    up_weight,
    down_weight,
    shared_gate,
    shared_up,
    shared_down,
):
    local_rows, top_count = expert_ids.shape
    local_experts = gate_weight.shape[0]
    ep_size = lax.axis_size("ep")
    experts_all = local_experts * ep_size
    capacity = 3 * local_rows * top_count // (2 * experts_all)
    model_width = expert_input.shape[1]
    lane_cols = model_width // lax.axis_size("tp")
    slots_total = ep_size * capacity
    widened = expert_input.astype(jnp.float32)
    normed = (
        widened
        * lax.rsqrt(jnp.mean(widened * widened, axis=1, keepdims=True) + EPSILON)
        * expert_gain
    ).astype(jnp.bfloat16)
    route_weight = gate_score / jnp.sum(gate_score, axis=1, keepdims=True) * ROUTED_SCALE
    pair_ids = expert_ids.reshape(local_rows * top_count)
    onehot = (pair_ids[:, None] == jnp.arange(experts_all, dtype=jnp.int32)).astype(jnp.int32)
    ranks = jnp.sum(
        (jnp.cumsum(onehot, axis=0, dtype=jnp.int32) - 1) * onehot, axis=1, dtype=jnp.int32
    )
    slot_index = pair_ids * capacity + ranks
    row_numbers = jnp.arange(local_rows * top_count, dtype=jnp.int32) // top_count
    sources = jnp.full((experts_all * capacity,), -1, jnp.int32).at[slot_index].set(row_numbers)
    filled = (sources >= 0)[:, None]
    safe_rows = jnp.maximum(sources, 0)
    nothing = jnp.zeros((), jnp.bfloat16)
    lane_start = lax.axis_index("tp") * lane_cols
    own_cols = lax.dynamic_slice_in_dim(normed, lane_start, lane_cols, 1)
    outgoing = jnp.where(filled, own_cols[safe_rows], nothing).reshape(
        experts_all, capacity, lane_cols
    )
    arrived = lax.all_to_all(outgoing, "ep", split_axis=0, concat_axis=0, tiled=True)
    arranged = arrived.reshape(ep_size, local_experts, capacity, lane_cols).transpose(1, 0, 2, 3)
    arranged = arranged.reshape(local_experts, slots_total, lane_cols)
    piece = lax.all_gather(arranged, "tp", axis=2, tiled=True)
    gate_value = jnp.einsum("esd,edf->esf", piece, gate_weight, preferred_element_type=jnp.float32)
    up_value = jnp.einsum("esd,edf->esf", piece, up_weight, preferred_element_type=jnp.float32)
    hidden = (jax.nn.silu(gate_value) * up_value).astype(jnp.bfloat16)
    down_part = jnp.einsum("esf,efd->esd", hidden, down_weight, preferred_element_type=jnp.float32)
    down_rows = down_part.reshape(local_experts, ep_size, capacity, model_width).transpose(
        1, 0, 2, 3
    )
    down_rows = down_rows.reshape(experts_all * capacity, model_width)
    shared_gate_value = jnp.dot(normed, shared_gate, preferred_element_type=jnp.float32)
    shared_up_value = jnp.dot(normed, shared_up, preferred_element_type=jnp.float32)
    shared_hidden = (jax.nn.silu(shared_gate_value) * shared_up_value).astype(jnp.bfloat16)
    shared_part = jnp.dot(shared_hidden, shared_down, preferred_element_type=jnp.float32)
    terms = jnp.concatenate([down_rows, shared_part], axis=0)
    summed = lax.psum_scatter(
        terms.astype(jnp.bfloat16), "tp", scatter_dimension=1, tiled=True
    ).astype(jnp.float32)
    routed_slots = (
        summed[: experts_all * capacity]
        .astype(jnp.bfloat16)
        .reshape(experts_all, capacity, lane_cols)
    )
    shared_cols = summed[experts_all * capacity :]
    returned = lax.all_to_all(routed_slots, "ep", split_axis=0, concat_axis=0, tiled=True)
    picked = returned.reshape(experts_all * capacity, lane_cols)[slot_index]
    picked = picked.reshape(local_rows, top_count, lane_cols)
    routed = jnp.sum(picked.astype(jnp.float32) * route_weight[:, :, None], axis=1)
    return (routed + shared_cols).astype(jnp.bfloat16)


def body(
    query_rows,
    key_rows,
    value_rows,
    query_gain,
    key_gain,
    out_weight,
    mixer_gain,
    expert_input,
    expert_ids,
    gate_score,
    expert_gain,
    gate_weight,
    up_weight,
    down_weight,
    shared_gate,
    shared_up,
    shared_down,
):
    mixer_out = mixer_half(
        query_rows, key_rows, value_rows, query_gain, key_gain, out_weight, mixer_gain
    )
    expert_out = expert_half(
        expert_input,
        expert_ids,
        gate_score,
        expert_gain,
        gate_weight,
        up_weight,
        down_weight,
        shared_gate,
        shared_up,
        shared_down,
    )
    return (mixer_out, expert_out)


def solution(mesh):
    in_specs = (
        P("ep", "tp"),
        P("ep", None),
        P("ep", None),
        P(),
        P(),
        P("tp", None),
        P(),
        P("ep", None),
        P("ep", None),
        P("ep", None),
        P(),
        P("ep", None, "tp"),
        P("ep", None, "tp"),
        P("ep", "tp", None),
        P(None, "tp"),
        P(None, "tp"),
        P("tp", None),
    )
    out_specs = (P("ep", None), P("ep", "tp"))
    return jax.shard_map(body, mesh=mesh, in_specs=in_specs, out_specs=out_specs, check_vma=False)
```

profile of v0, /device:TPU:0, one launch (start us, length us, event | category | flops | bytes accessed | tf_op | source)
XLA Modules:
  0.0 218.4 jit_solution(9273533455983463291)
XLA Ops:
  7.2 1.0 copy.49
  9.2 1.1 reduce-window.6
  11.0 2.4 %scatter_custom_fusion = s32[768]{0:T(1024)S(1)} fusion(s32[512]{0:T(512)S(1)} %bitcast.141, s32[512]{0:T(512)S(1)} %add_select_fusion, s32[]{:T(128)} %constant.116.clone.1), kind=kCustom, calls=%fused_computation.114 | custom fusion | bytes 3076 | tf_op jit(solution)/shard_map/scatter | solution.py:141
  13.5 1.5 fusion.26
  15.1 1.0 fusion.28
  16.2 1.0 copy-done.4
  17.1 2.7 %gather_fusion = bf16[768,512]{1,0:T(8,128)(2,1)S(1)} fusion(bf16[256,512]{1,0:T(8,128)(2,1)S(1)} %constant_dynamic-slice_fusion.1, s32[1024]{0:T(1024)S(1)} %pad_clamp_fusion.1), kind=kCustom, calls=%fused_computation | custom fusion | bytes 1575936 | tf_op jit(solution)/shard_map/gather | solution.py:147
  20.0 27.3 %all_to_all.10 = bf16[8,96,512]{2,1,0:T(8,128)(2,1)} all-to-all(bf16[8,96,512]{2,1,0:T(8,128)(2,1)S(1)} %broadcast_select_fusion), channel_id=1, replica_groups=mesh['ep'=8,'tp'=4] {'ep'}, dimensions={0} | all-to-all | bytes 1572864 | tf_op jit(solution)/shard_map/all_to_all | solution.py:150
  47.5 1.1 constant_dynamic-slice_fusion.2
  50.8 3.1 %fusion.67 = f32[256,512]{1,0:T(8,128)} fusion(bf16[256,2048]{1,0:T(8,128)(2,1)S(1)} %copy-done.5, bf16[2048,512]{1,0:T(8,128)(2,1)} %param.33), kind=kOutput, calls=%fused_computation.131 | convolution fusion | flops 536870912 | bytes 3670016 | tf_op jit(solution)/shard_map/dot_general | solution.py:162
  53.9 34.3 %all_gather.6 = bf16[3072,128]{1,0:T(8,128)(2,1)} all-gather(bf16[384,128]{1,0:T(8,128)(2,1)S(1)} %pad_maximum_fusion.2), channel_id=1, replica_groups=mesh['ep'=8,'tp'=4] {'ep'}, dimensions={0}, use_global_device_ids=true | all-gather | bytes 884736 | tf_op jit(solution)/shard_map/all_gather | solution.py:90
  88.1 4.3 %convolution_convert_fusion = bf16[256,2048]{1,0:T(8,128)(2,1)} fusion(bf16[512,2048]{1,0:T(8,128)(2,1)S(1)} %copy-done, bf16[256,2048]{1,0:T(8,128)(2,1)} %copy-done.4, bf16[2048,512]{1,0:T(8,128)(2,1)} %param.34, f32[256,512]{1,0:T(8,128)} %fusion.67), kind=kOutput, calls=%fused_computation.44 | convolution fusion | flops 1075052544 | bytes 6815744 | tf_op jit(solution)/shard_map/dot_general | solution.py:165
  92.5 6.3 %fusion.16 = f32[768,1024]{1,0:T(8,128)S(1)} fusion(bf16[1,2048,1024]{2,1,0:T(8,128)(2,1)} %param.30, bf16[1,768,2048]{2,1,0:T(8,128)(2,1)} %all-gather.2.cloned.1.call-done), kind=kOutput, calls=%fused_computation.30 | convolution fusion | flops 3221225472 | bytes 10485760 | tf_op jit(solution)/shard_map/esd,edf->esf/dot_general | solution.py:154
  98.8 3.6 %multiply_convert_fusion = bf16[768,1024]{1,0:T(8,128)(2,1)S(1)} fusion(f32[768,1024]{1,0:T(8,128)S(1)} %fusion.16, bf16[1,2048,1024]{2,1,0:T(8,128)(2,1)S(1)} %copy-done.12, bf16[1,768,2048]{2,1,0:T(8,128)(2,1)S(1)} %copy-done.14), kind=kOutput, calls=%fused_computation.41 | convolution fusion | flops 3225944064 | bytes 12058624 | tf_op jit(solution)/shard_map/esd,edf->esf/dot_general | solution.py:155
  102.4 3.6 %fusion.18 = bf16[768,2048]{1,0:T(8,128)(2,1)S(1)} fusion(bf16[768,1024]{1,0:T(8,128)(2,1)S(1)} %multiply_convert_fusion, bf16[1,1024,2048]{2,1,0:T(8,128)(2,1)S(1)} %copy-done.13), kind=kOutput, calls=%fused_computation.34 | convolution fusion | flops 3222798336 | bytes 8912896 | tf_op jit(solution)/shard_map/esf,efd->esd/dot_general | solution.py:157
  106.1 2.2 %pad_maximum_fusion = bf16[1024,2048]{1,0:T(8,128)(2,1)} fusion(bf16[256,2048]{1,0:T(8,128)(2,1)S(1)} %copy-done.6, bf16[768,2048]{1,0:T(8,128)(2,1)S(1)} %fusion.18), kind=kLoop, calls=%fused_computation.25 | loop fusion | flops 8388608 | bytes 8388608 | tf_op jit(solution)/shard_map/concatenate | solution.py:166
  108.4 47.6 %while.15 = (s32[]{:T(128)}, f32[1,4,384]{2,1,0:T(4,128)S(1)}, f32[1,4,384]{2,1,0:T(4,128)S(1)}, f32[1,4,384,64]{2,3,1,0:T(8,128)S(1)}, bf16[8,384,128]{2,1,0:T(...) while((s32[]{:T(128)}, f32[1,4,384]{2,1,0:T(4,128)S(1)}, ...), condition=%wide.region_5.6_spmd.clone, body=%wide.region_2.5_spmd.clone.sunk | while | flops 156017664 | bytes 18088064 | solution.py:95
  108.4 0.9 constant_dynamic-slice_fusion.5
  109.4 1.9 bitcast_reduce_fusion.2
  111.3 2.8 %fusion.82 = f32[1,4,384,64]{2,3,1,0:T(8,128)S(1)} fusion(f32[384,384,4]{1,0,2:T(8,128)} %get-tuple-element.151, f32[4,384]{1,0:T(4,128)S(1)} %bitcast.134, f32[1,4,384,64]{2,3,1,0:T(8,128)S(1)} %get-tuple-element.164, f32[4,384]{1,0:T(4,128)S(1)} %get-tuple-element.152, pred[]{:T(512)S(6)} %compare.18, bf16[384,128]{0,1:T(8,128)(2,1)S(1)} %bitcast.133), kind=kOutput, calls=%fused_computation.9.clone.1 | convolution fusion | flops 77561856 | bytes 3207169 | tf_op jit(solution)/shard_map/while/body/eval_jaxpr/kgqs,skd->kgqd/dot_general | solution.py:76
  114.8 0.9 constant_dynamic-slice_fusion.5
  115.9 1.9 bitcast_reduce_fusion.2
  117.8 2.5 %fusion.82 = f32[1,4,384,64]{2,3,1,0:T(8,128)S(1)} fusion(f32[384,384,4]{1,0,2:T(8,128)} %get-tuple-element.151, f32[4,384]{1,0:T(4,128)S(1)} %bitcast.134, f32[1,4,384,64]{2,3,1,0:T(8,128)S(1)} %get-tuple-element.164, f32[4,384]{1,0:T(4,128)S(1)} %get-tuple-element.152, pred[]{:T(512)S(6)} %compare.18, bf16[384,128]{0,1:T(8,128)(2,1)S(1)} %bitcast.133), kind=kOutput, calls=%fused_computation.9.clone.1 | convolution fusion | flops 77561856 | bytes 3207169 | tf_op jit(solution)/shard_map/while/body/eval_jaxpr/kgqs,skd->kgqd/dot_general | solution.py:76
  120.8 0.9 constant_dynamic-slice_fusion.5
  121.8 1.9 bitcast_reduce_fusion.2
  123.7 2.4 %fusion.82 = f32[1,4,384,64]{2,3,1,0:T(8,128)S(1)} fusion(f32[384,384,4]{1,0,2:T(8,128)} %get-tuple-element.151, f32[4,384]{1,0:T(4,128)S(1)} %bitcast.134, f32[1,4,384,64]{2,3,1,0:T(8,128)S(1)} %get-tuple-element.164, f32[4,384]{1,0:T(4,128)S(1)} %get-tuple-element.152, pred[]{:T(512)S(6)} %compare.18, bf16[384,128]{0,1:T(8,128)(2,1)S(1)} %bitcast.133), kind=kOutput, calls=%fused_computation.9.clone.1 | convolution fusion | flops 77561856 | bytes 3207169 | tf_op jit(solution)/shard_map/while/body/eval_jaxpr/kgqs,skd->kgqd/dot_general | solution.py:76
  126.8 0.9 constant_dynamic-slice_fusion.5
  127.8 1.9 bitcast_reduce_fusion.2
  129.8 2.4 %fusion.82 = f32[1,4,384,64]{2,3,1,0:T(8,128)S(1)} fusion(f32[384,384,4]{1,0,2:T(8,128)} %get-tuple-element.151, f32[4,384]{1,0:T(4,128)S(1)} %bitcast.134, f32[1,4,384,64]{2,3,1,0:T(8,128)S(1)} %get-tuple-element.164, f32[4,384]{1,0:T(4,128)S(1)} %get-tuple-element.152, pred[]{:T(512)S(6)} %compare.18, bf16[384,128]{0,1:T(8,128)(2,1)S(1)} %bitcast.133), kind=kOutput, calls=%fused_computation.9.clone.1 | convolution fusion | flops 77561856 | bytes 3207169 | tf_op jit(solution)/shard_map/while/body/eval_jaxpr/kgqs,skd->kgqd/dot_general | solution.py:76
  133.7 1.9 bitcast_reduce_fusion.2
  135.6 2.4 %fusion.82 = f32[1,4,384,64]{2,3,1,0:T(8,128)S(1)} fusion(f32[384,384,4]{1,0,2:T(8,128)} %get-tuple-element.151, f32[4,384]{1,0:T(4,128)S(1)} %bitcast.134, f32[1,4,384,64]{2,3,1,0:T(8,128)S(1)} %get-tuple-element.164, f32[4,384]{1,0:T(4,128)S(1)} %get-tuple-element.152, pred[]{:T(512)S(6)} %compare.18, bf16[384,128]{0,1:T(8,128)(2,1)S(1)} %bitcast.133), kind=kOutput, calls=%fused_computation.9.clone.1 | convolution fusion | flops 77561856 | bytes 3207169 | tf_op jit(solution)/shard_map/while/body/eval_jaxpr/kgqs,skd->kgqd/dot_general | solution.py:76
  138.4 0.9 constant_dynamic-slice_fusion.5
  139.5 1.9 bitcast_reduce_fusion.2
  141.4 2.4 %fusion.82 = f32[1,4,384,64]{2,3,1,0:T(8,128)S(1)} fusion(f32[384,384,4]{1,0,2:T(8,128)} %get-tuple-element.151, f32[4,384]{1,0:T(4,128)S(1)} %bitcast.134, f32[1,4,384,64]{2,3,1,0:T(8,128)S(1)} %get-tuple-element.164, f32[4,384]{1,0:T(4,128)S(1)} %get-tuple-element.152, pred[]{:T(512)S(6)} %compare.18, bf16[384,128]{0,1:T(8,128)(2,1)S(1)} %bitcast.133), kind=kOutput, calls=%fused_computation.9.clone.1 | convolution fusion | flops 77561856 | bytes 3207169 | tf_op jit(solution)/shard_map/while/body/eval_jaxpr/kgqs,skd->kgqd/dot_general | solution.py:76
  145.3 1.9 bitcast_reduce_fusion.2
  147.2 2.4 %fusion.82 = f32[1,4,384,64]{2,3,1,0:T(8,128)S(1)} fusion(f32[384,384,4]{1,0,2:T(8,128)} %get-tuple-element.151, f32[4,384]{1,0:T(4,128)S(1)} %bitcast.134, f32[1,4,384,64]{2,3,1,0:T(8,128)S(1)} %get-tuple-element.164, f32[4,384]{1,0:T(4,128)S(1)} %get-tuple-element.152, pred[]{:T(512)S(6)} %compare.18, bf16[384,128]{0,1:T(8,128)(2,1)S(1)} %bitcast.133), kind=kOutput, calls=%fused_computation.9.clone.1 | convolution fusion | flops 77561856 | bytes 3207169 | tf_op jit(solution)/shard_map/while/body/eval_jaxpr/kgqs,skd->kgqd/dot_general | solution.py:76
  151.1 1.9 bitcast_reduce_fusion.2
  153.1 2.4 %fusion.82 = f32[1,4,384,64]{2,3,1,0:T(8,128)S(1)} fusion(f32[384,384,4]{1,0,2:T(8,128)} %get-tuple-element.151, f32[4,384]{1,0:T(4,128)S(1)} %bitcast.134, f32[1,4,384,64]{2,3,1,0:T(8,128)S(1)} %get-tuple-element.164, f32[4,384]{1,0:T(4,128)S(1)} %get-tuple-element.152, pred[]{:T(512)S(6)} %compare.18, bf16[384,128]{0,1:T(8,128)(2,1)S(1)} %bitcast.133), kind=kOutput, calls=%fused_computation.9.clone.1 | convolution fusion | flops 77561856 | bytes 3207169 | tf_op jit(solution)/shard_map/while/body/eval_jaxpr/kgqs,skd->kgqd/dot_general | solution.py:76
  155.9 3.0 %bitcast_convert_fusion = bf16[384,2048]{1,0:T(8,128)(2,1)} fusion(bf16[4,64,2048]{2,1,0:T(8,128)(2,1)} %bitcast.144, f32[1,4,384,64]{2,3,1,0:T(8,128)S(1)} %get-tuple-element.35, f32[4,384]{1,0:T(4,128)S(1)} %bitcast.140), kind=kOutput, calls=%fused_computation.40 | convolution fusion | flops 403636224 | bytes 3020800 | tf_op jit(solution)/shard_map/kgqd,kgde->qe/dot_general | solution.py:99
  159.0 2.1 slice.56
  161.0 3.8 %all-to-all-start.1 = ((bf16[8,96,512]{2,1,0:T(8,128)(2,1)}), bf16[8,96,512]{2,1,0:T(8,128)(2,1)S(1)}, u32[]{:S(2)}, u32[]{:S(2)}) async-start(bf16[8,96,512]{2,1,0:T(8,128)(2,1)} %bitcast.137), calls=%async_computation.2 | async-start | bytes 1572864 | tf_op jit(solution)/shard_map/all_to_all | solution.py:176
  165.0 35.9 %all-reduce.2.cloned.1.call-done = bf16[384,2048]{1,0:T(8,128)(2,1)} async-done(((bf16[384,2048]{1,0:T(8,128)(2,1)}), bf16[384,2048]{1,0:T(8,128)(2,1)}) %all-reduce.2.cloned.1.call-update) | async-done | bytes 1572880 | tf_op jit(solution)/shard_map/psum | solution.py:102
  200.9 1.9 fusion.21
  202.9 1.6 fusion.23
  204.5 2.6 %gather_fusion.1 = bf16[512,512]{1,0:T(8,128)(2,1)} fusion(bf16[768,512]{1,0:T(8,128)(2,1)S(1)} %bitcast.131, s32[1024]{0:T(1024)S(1)} %pad_clamp_fusion), kind=kCustom, calls=%fused_computation.1 | custom fusion | bytes 1050624 | tf_op jit(solution)/shard_map/gather | solution.py:177
  207.1 1.7 reshape.421
  208.8 1.3 multiply_reduce_fusion
  210.1 1.7 add_convert_fusion
  (140 shorter events, 12.1 us)
Async XLA Ops:
  7.2 81.0 %copy-start = (bf16[512,2048]{1,0:T(8,128)(2,1)S(1)}, bf16[512,2048]{1,0:T(8,128)(2,1)}, u32[]{:S(2)}) copy-start(bf16[512,2048]{1,0:T(8,128)(2,1)} %param.35) | copy-start | bytes 6291460
  7.2 8.0 %copy-start.3 = (bf16[256,2048]{1,0:T(8,128)(2,1)S(1)}, bf16[256,2048]{1,0:T(8,128)(2,1)}, u32[]{:S(2)}) copy-start(bf16[256,2048]{1,0:T(8,128)(2,1)} %param.26) | copy-start | bytes 3145732
  7.2 85.3 %all-gather.2.cloned.1.call-start = ((), (), s32[]{:S(2)}) async-start(), calls=%async_computation.4 | async-start | bytes 3932160 | tf_op jit(solution)/shard_map/all_gather | solution.py:153
  16.1 1.0 copy-start.4
  19.8 29.0 %copy-start.10 = (f32[64]{0:T(128)S(1)}, f32[64]{0:T(128)}, u32[]{:S(2)}) copy-start(f32[64]{0:T(128)} %param.23) | copy-start | bytes 772
  19.8 29.5 %copy-start.7 = (bf16[384,256]{1,0:T(8,128)(2,1)S(1)}, bf16[384,256]{1,0:T(8,128)(2,1)}, u32[]{:S(2)}) copy-start(bf16[384,256]{1,0:T(8,128)(2,1)} %param.19) | copy-start | bytes 589828
  20.0 29.9 %copy-start.11 = (f32[64]{0:T(128)S(1)}, f32[64]{0:T(128)}, u32[]{:S(2)}) copy-start(f32[64]{0:T(128)} %param.22) | copy-start | bytes 772
  47.4 111.6 %reduce-scatter.2.cloned.1.call-start = ((), (), s32[]{:S(2)}) async-start(), calls=%async_computation.5 | async-start | bytes 5242880 | tf_op jit(solution)/shard_map/reduce_scatter | solution.py:167
  49.5 1.2 copy-start.5
  92.5 6.3 %copy-start.12 = (bf16[1,2048,1024]{2,1,0:T(8,128)(2,1)S(1)}, bf16[1,2048,1024]{2,1,0:T(8,128)(2,1)}, u32[]{:S(2)}) copy-start(bf16[1,2048,1024]{2,1,0:T(8,128)(2,1)} %param.31) | copy-start | bytes 12582916
  92.5 6.3 %copy-start.14 = (bf16[1,768,2048]{2,1,0:T(8,128)(2,1)S(1)}, bf16[1,768,2048]{2,1,0:T(8,128)(2,1)}, u32[]{:S(2)}) copy-start(bf16[1,768,2048]{2,1,0:T(8,128)(2,1)} %all-gather.2.cloned.1.call-done) | copy-start | bytes 9437188
  98.8 3.6 %copy-start.13 = (bf16[1,1024,2048]{2,1,0:T(8,128)(2,1)S(1)}, bf16[1,1024,2048]{2,1,0:T(8,128)(2,1)}, u32[]{:S(2)}) copy-start(bf16[1,1024,2048]{2,1,0:T(8,128)(2,1)} %param.32) | copy-start | bytes 12582916
  102.4 3.6 %copy-start.6 = (bf16[256,2048]{1,0:T(8,128)(2,1)S(1)}, bf16[256,2048]{1,0:T(8,128)(2,1)}, u32[]{:S(2)}) copy-start(bf16[256,2048]{1,0:T(8,128)(2,1)} %convolution_convert_fusion) | copy-start | bytes 3145732
  108.3 92.6 %all-reduce.2.cloned.1.call-start = ((), (), s32[]{:S(2)}) async-start(), calls=%async_computation.3 | async-start | bytes 3145728 | tf_op jit(solution)/shard_map/psum | solution.py:102
  111.3 3.1 %copy-start.1 = (f32[384,384,4]{1,0,2:T(8,128)S(1)}, f32[384,384,4]{1,0,2:T(8,128)}, u32[]{:S(2)}) copy-start(f32[384,384,4]{1,0,2:T(8,128)} %get-tuple-element.151) | copy-start | bytes 7077892 | tf_op jit(solution)/shard_map/while
  117.8 2.5 %copy-start.1 = (f32[384,384,4]{1,0,2:T(8,128)S(1)}, f32[384,384,4]{1,0,2:T(8,128)}, u32[]{:S(2)}) copy-start(f32[384,384,4]{1,0,2:T(8,128)} %get-tuple-element.151) | copy-start | bytes 7077892 | tf_op jit(solution)/shard_map/while
  123.7 2.6 %copy-start.1 = (f32[384,384,4]{1,0,2:T(8,128)S(1)}, f32[384,384,4]{1,0,2:T(8,128)}, u32[]{:S(2)}) copy-start(f32[384,384,4]{1,0,2:T(8,128)} %get-tuple-element.151) | copy-start | bytes 7077892 | tf_op jit(solution)/shard_map/while
  129.7 2.4 %copy-start.1 = (f32[384,384,4]{1,0,2:T(8,128)S(1)}, f32[384,384,4]{1,0,2:T(8,128)}, u32[]{:S(2)}) copy-start(f32[384,384,4]{1,0,2:T(8,128)} %get-tuple-element.151) | copy-start | bytes 7077892 | tf_op jit(solution)/shard_map/while
  135.6 2.4 %copy-start.1 = (f32[384,384,4]{1,0,2:T(8,128)S(1)}, f32[384,384,4]{1,0,2:T(8,128)}, u32[]{:S(2)}) copy-start(f32[384,384,4]{1,0,2:T(8,128)} %get-tuple-element.151) | copy-start | bytes 7077892 | tf_op jit(solution)/shard_map/while
  141.4 2.4 %copy-start.1 = (f32[384,384,4]{1,0,2:T(8,128)S(1)}, f32[384,384,4]{1,0,2:T(8,128)}, u32[]{:S(2)}) copy-start(f32[384,384,4]{1,0,2:T(8,128)} %get-tuple-element.151) | copy-start | bytes 7077892 | tf_op jit(solution)/shard_map/while
  147.2 2.4 %copy-start.1 = (f32[384,384,4]{1,0,2:T(8,128)S(1)}, f32[384,384,4]{1,0,2:T(8,128)}, u32[]{:S(2)}) copy-start(f32[384,384,4]{1,0,2:T(8,128)} %get-tuple-element.151) | copy-start | bytes 7077892 | tf_op jit(solution)/shard_map/while
  153.1 2.4 %copy-start.1 = (f32[384,384,4]{1,0,2:T(8,128)S(1)}, f32[384,384,4]{1,0,2:T(8,128)}, u32[]{:S(2)}) copy-start(f32[384,384,4]{1,0,2:T(8,128)} %get-tuple-element.151) | copy-start | bytes 7077892 | tf_op jit(solution)/shard_map/while
  158.9 5.9 %copy-start.9 = (f32[256,2]{0,1:T(2,128)S(1)}, f32[256,2]{0,1:T(2,128)}, u32[]{:S(2)}) copy-start(f32[256,2]{0,1:T(2,128)} %param.28) | copy-start | bytes 6148
  158.9 43.9 %copy-start.8 = (f32[2048]{0:T(1024)S(1)}, f32[2048]{0:T(1024)}, u32[]{:S(2)}) copy-start(f32[2048]{0:T(1024)} %param.25) | copy-start | bytes 24580
  161.0 43.4 %all-to-all-start.1 = ((bf16[8,96,512]{2,1,0:T(8,128)(2,1)}), bf16[8,96,512]{2,1,0:T(8,128)(2,1)S(1)}, u32[]{:S(2)}, u32[]{:S(2)}) async-start(bf16[8,96,512]{2,1,0:T(8,128)(2,1)} %bitcast.137), calls=%async_computation.2 | async-start | bytes 1572864 | tf_op jit(solution)/shard_map/all_to_all | solution.py:176
  200.9 1.9 copy-start.2
Sparse Core Ops, SparseCore 0:
  47.5 27.5 all-gather.1
  108.4 43.3 reduce-scatter.1
  159.1 41.8 all-reduce.1
where the time goes:
time: 219 us; the launch traced here: 218 us
  blocking collectives  61.6 us (28%)
  matrix products  58.9 us (27%)
  waiting for transfers between devices  36 us (16%)
  local copies, waits for them, and re-layouts  25.5 us (12%)
  other arithmetic  17.9 us (8%)
  between operations  14.2 us (6%)
  starting transfers between devices  3.9 us (2%)
    psum x1, waiting for transfers between devices, mixer_half(): lax.psum(partial_value.astype(jnp.bfloat16), 'tp').astype(jnp.float32)  35.9 us
    all_gather x1, blocking collectives, mixer_half(): piece = lax.all_gather(stacked, 'ep', axis=0, tiled=True)  34.3 us
    all_to_all x1, blocking collectives, expert_half(): lax.all_to_all(outgoing, 'ep', split_axis=0, concat_axis=0, tiled=True)  27.3 us
    dot_general x8, matrix products, step_block(): jnp.einsum('kgqs,skd->kgqd', exponent.astype(jnp.bfloat16), block_values,...  19.6 us
    dot_general x8, matrix products, step_block(): jnp.einsum('qkgd,skd->kgqs', query_grouped, block_keys, preferred_element...  15.3 us
    dynamic_slice x16, local copies, waits for them, and re-layouts, mixer_half(): carry, unused = lax.scan(step_block, carry, blocks)  8.26 us
    dot_general x1, matrix products, expert_half(): jnp.einsum('esd,edf->esf', piece, gate_weight, preferred_element_type=jnp...  6.28 us
  transfers between devices with their start and end apart: 4, of which 1 were waited for; matrix products, arithmetic and copies ran while one was open for 30% of the time, Pallas kernels for 0%

commit v1 on v0

--- a/solution.py
+++ b/solution.py
@@ -3,6 +3,7 @@
 import jax.numpy as jnp
 from jax import lax
 from jax.sharding import PartitionSpec as P
+from jax.lax import all_gather
 
 HEADS = 16
 KV_HEADS = 4
@@ -99,7 +100,9 @@
     partial_value = jnp.einsum(
         "kgqd,kgde->qe", attended, lane_weight, preferred_element_type=jnp.float32
     )
-    mixer_sum = lax.psum(partial_value.astype(jnp.bfloat16), "tp").astype(jnp.float32)
+    mixer_sum = jnp.sum(all_gather(partial_value.astype(jnp.bfloat16), "tp"), axis=0).astype(
+        jnp.float32
+    )
     mixer_scale = lax.rsqrt(jnp.mean(mixer_sum * mixer_sum, axis=1, keepdims=True) + EPSILON)
     return (mixer_sum * mixer_scale * mixer_gain).astype(jnp.bfloat16)
 

time: 219 us -> 228 us (1.041)
  other arithmetic: 17.9 us -> 23.7 us
  waiting for transfers between devices: 36 us -> 39.5 us
    all_gather x0 -> x1, waiting for transfers between devices: none -> 39.5 us  [mixer_half(): all_gather(partial_value.astype(jnp.bfloat16), 'tp')]
    psum x1 -> x0, waiting for transfers between devices: 35.9 us -> none  [mixer_half(): lax.psum(partial_value.astype(jnp.bfloat16), 'tp').astype(jnp.float32)]
    reduce_sum x0 -> x1, other arithmetic: none -> 5.66 us  [mixer_half(): jnp.sum(all_gather(partial_value.astype(jnp.bfloat16), 'tp'), axis=0)]
  transfers between devices with their start and end apart: 4 -> 4, of which waited for: 1 -> 1; matrix products, arithmetic and copies ran while one was open for 30% -> 31% of each run, Pallas kernels for 0% -> 0%
where the time goes in v1:
time: 228 us
  blocking collectives  61.6 us (27%)
  matrix products  58.8 us (26%)
  waiting for transfers between devices  39.5 us (17%)
  local copies, waits for them, and re-layouts  25.5 us (11%)
  other arithmetic  23.7 us (10%)
  between operations  14.2 us (6%)
  starting transfers between devices  3.91 us (2%)
    all_gather x1, waiting for transfers between devices, mixer_half(): all_gather(partial_value.astype(jnp.bfloat16), 'tp')  39.5 us
    all_gather x1, blocking collectives, mixer_half(): piece = lax.all_gather(stacked, 'ep', axis=0, tiled=True)  34.3 us
    all_to_all x1, blocking collectives, expert_half(): lax.all_to_all(outgoing, 'ep', split_axis=0, concat_axis=0, tiled=True)  27.3 us
    dot_general x8, matrix products, step_block(): jnp.einsum('kgqs,skd->kgqd', exponent.astype(jnp.bfloat16), block_values,...  19.6 us
    dot_general x8, matrix products, step_block(): jnp.einsum('qkgd,skd->kgqs', query_grouped, block_keys, preferred_element...  15.3 us
    dynamic_slice x16, local copies, waits for them, and re-layouts, mixer_half(): carry, unused = lax.scan(step_block, carry, blocks)  8.25 us
    dot_general x1, matrix products, expert_half(): jnp.einsum('esd,edf->esf', piece, gate_weight, preferred_element_type=jnp...  6.28 us
    reduce_sum x1, other arithmetic, mixer_half(): jnp.sum(all_gather(partial_value.astype(jnp.bfloat16), 'tp'), axis=0)  5.66 us
  transfers between devices with their start and end apart: 4, of which 1 were waited for; matrix products, arithmetic and copies ran while one was open for 31% of the time, Pallas kernels for 0%

profile of v1, /device:TPU:0, one launch (start us, length us, event | category | flops | bytes accessed | tf_op | source)
XLA Modules:
  0.0 227.6 jit_solution(15658847584594740488)
XLA Ops:
  7.2 1.0 copy.49
  9.2 1.1 reduce-window.6
  11.0 2.4 %scatter_custom_fusion = s32[768]{0:T(1024)S(1)} fusion(s32[512]{0:T(512)S(1)} %bitcast.143, s32[512]{0:T(512)S(1)} %add_select_fusion, s32[]{:T(128)} %constant.117.clone.1), kind=kCustom, calls=%fused_computation.114 | custom fusion | bytes 3076 | tf_op jit(solution)/shard_map/scatter | solution.py:144
  13.5 1.5 fusion.26
  15.1 1.0 fusion.28
  16.2 1.0 copy-done.4
  17.1 2.7 %gather_fusion = bf16[768,512]{1,0:T(8,128)(2,1)S(1)} fusion(bf16[256,512]{1,0:T(8,128)(2,1)S(1)} %constant_dynamic-slice_fusion.1, s32[1024]{0:T(1024)S(1)} %pad_clamp_fusion.1), kind=kCustom, calls=%fused_computation | custom fusion | bytes 1575936 | tf_op jit(solution)/shard_map/gather | solution.py:150
  20.0 27.3 %all_to_all.10 = bf16[8,96,512]{2,1,0:T(8,128)(2,1)} all-to-all(bf16[8,96,512]{2,1,0:T(8,128)(2,1)S(1)} %broadcast_select_fusion), channel_id=1, replica_groups=mesh['ep'=8,'tp'=4] {'ep'}, dimensions={0} | all-to-all | bytes 1572864 | tf_op jit(solution)/shard_map/all_to_all | solution.py:153
  47.5 1.1 constant_dynamic-slice_fusion.2
  50.8 3.1 %fusion.67 = f32[256,512]{1,0:T(8,128)} fusion(bf16[256,2048]{1,0:T(8,128)(2,1)S(1)} %copy-done.5, bf16[2048,512]{1,0:T(8,128)(2,1)} %param.33), kind=kOutput, calls=%fused_computation.131 | convolution fusion | flops 536870912 | bytes 3670016 | tf_op jit(solution)/shard_map/dot_general | solution.py:165
  53.9 34.3 %all_gather.12 = bf16[3072,128]{1,0:T(8,128)(2,1)} all-gather(bf16[384,128]{1,0:T(8,128)(2,1)S(1)} %pad_maximum_fusion.2), channel_id=1, replica_groups=mesh['ep'=8,'tp'=4] {'ep'}, dimensions={0}, use_global_device_ids=true | all-gather | bytes 884736 | tf_op jit(solution)/shard_map/all_gather | solution.py:91
  88.1 4.3 %convolution_convert_fusion = bf16[256,2048]{1,0:T(8,128)(2,1)} fusion(bf16[512,2048]{1,0:T(8,128)(2,1)S(1)} %copy-done, bf16[256,2048]{1,0:T(8,128)(2,1)} %copy-done.4, bf16[2048,512]{1,0:T(8,128)(2,1)} %param.34, f32[256,512]{1,0:T(8,128)} %fusion.67), kind=kOutput, calls=%fused_computation.44 | convolution fusion | flops 1075052544 | bytes 6815744 | tf_op jit(solution)/shard_map/dot_general | solution.py:168
  92.5 6.3 %fusion.16 = f32[768,1024]{1,0:T(8,128)S(1)} fusion(bf16[1,2048,1024]{2,1,0:T(8,128)(2,1)} %param.30, bf16[1,768,2048]{2,1,0:T(8,128)(2,1)} %all-gather.4.cloned.1.call-done), kind=kOutput, calls=%fused_computation.30 | convolution fusion | flops 3221225472 | bytes 10485760 | tf_op jit(solution)/shard_map/esd,edf->esf/dot_general | solution.py:157
  98.8 3.6 %multiply_convert_fusion = bf16[768,1024]{1,0:T(8,128)(2,1)S(1)} fusion(f32[768,1024]{1,0:T(8,128)S(1)} %fusion.16, bf16[1,2048,1024]{2,1,0:T(8,128)(2,1)S(1)} %copy-done.12, bf16[1,768,2048]{2,1,0:T(8,128)(2,1)S(1)} %copy-done.14), kind=kOutput, calls=%fused_computation.41 | convolution fusion | flops 3225944064 | bytes 12058624 | tf_op jit(solution)/shard_map/esd,edf->esf/dot_general | solution.py:158
  102.4 3.6 %fusion.18 = bf16[768,2048]{1,0:T(8,128)(2,1)S(1)} fusion(bf16[768,1024]{1,0:T(8,128)(2,1)S(1)} %multiply_convert_fusion, bf16[1,1024,2048]{2,1,0:T(8,128)(2,1)S(1)} %copy-done.13), kind=kOutput, calls=%fused_computation.34 | convolution fusion | flops 3222798336 | bytes 8912896 | tf_op jit(solution)/shard_map/esf,efd->esd/dot_general | solution.py:160
  106.1 2.3 %pad_maximum_fusion = bf16[1024,2048]{1,0:T(8,128)(2,1)} fusion(bf16[256,2048]{1,0:T(8,128)(2,1)S(1)} %copy-done.6, bf16[768,2048]{1,0:T(8,128)(2,1)S(1)} %fusion.18), kind=kLoop, calls=%fused_computation.25 | loop fusion | flops 8388608 | bytes 8388608 | tf_op jit(solution)/shard_map/concatenate | solution.py:169
  108.5 47.5 %while.15 = (s32[]{:T(128)}, f32[1,4,384]{2,1,0:T(4,128)S(1)}, f32[1,4,384]{2,1,0:T(4,128)S(1)}, f32[1,4,384,64]{2,3,1,0:T(8,128)S(1)}, bf16[8,384,128]{2,1,0:T(...) while((s32[]{:T(128)}, f32[1,4,384]{2,1,0:T(4,128)S(1)}, ...), condition=%wide.region_5.6_spmd.clone, body=%wide.region_2.5_spmd.clone.sunk | while | flops 156017664 | bytes 18088064 | solution.py:96
  108.5 0.9 constant_dynamic-slice_fusion.5
  109.5 1.9 bitcast_reduce_fusion.2
  111.5 2.8 %fusion.82 = f32[1,4,384,64]{2,3,1,0:T(8,128)S(1)} fusion(f32[384,384,4]{1,0,2:T(8,128)} %get-tuple-element.151, f32[4,384]{1,0:T(4,128)S(1)} %bitcast.136, f32[1,4,384,64]{2,3,1,0:T(8,128)S(1)} %get-tuple-element.164, f32[4,384]{1,0:T(4,128)S(1)} %get-tuple-element.152, pred[]{:T(512)S(6)} %compare.18, bf16[384,128]{0,1:T(8,128)(2,1)S(1)} %bitcast.134), kind=kOutput, calls=%fused_computation.9.clone.1 | convolution fusion | flops 77561856 | bytes 3207169 | tf_op jit(solution)/shard_map/while/body/eval_jaxpr/kgqs,skd->kgqd/dot_general | solution.py:77
  115.0 0.9 constant_dynamic-slice_fusion.5
  116.0 1.9 bitcast_reduce_fusion.2
  117.9 2.5 %fusion.82 = f32[1,4,384,64]{2,3,1,0:T(8,128)S(1)} fusion(f32[384,384,4]{1,0,2:T(8,128)} %get-tuple-element.151, f32[4,384]{1,0:T(4,128)S(1)} %bitcast.136, f32[1,4,384,64]{2,3,1,0:T(8,128)S(1)} %get-tuple-element.164, f32[4,384]{1,0:T(4,128)S(1)} %get-tuple-element.152, pred[]{:T(512)S(6)} %compare.18, bf16[384,128]{0,1:T(8,128)(2,1)S(1)} %bitcast.134), kind=kOutput, calls=%fused_computation.9.clone.1 | convolution fusion | flops 77561856 | bytes 3207169 | tf_op jit(solution)/shard_map/while/body/eval_jaxpr/kgqs,skd->kgqd/dot_general | solution.py:77
  121.9 1.9 bitcast_reduce_fusion.2
  123.8 2.4 %fusion.82 = f32[1,4,384,64]{2,3,1,0:T(8,128)S(1)} fusion(f32[384,384,4]{1,0,2:T(8,128)} %get-tuple-element.151, f32[4,384]{1,0:T(4,128)S(1)} %bitcast.136, f32[1,4,384,64]{2,3,1,0:T(8,128)S(1)} %get-tuple-element.164, f32[4,384]{1,0:T(4,128)S(1)} %get-tuple-element.152, pred[]{:T(512)S(6)} %compare.18, bf16[384,128]{0,1:T(8,128)(2,1)S(1)} %bitcast.134), kind=kOutput, calls=%fused_computation.9.clone.1 | convolution fusion | flops 77561856 | bytes 3207169 | tf_op jit(solution)/shard_map/while/body/eval_jaxpr/kgqs,skd->kgqd/dot_general | solution.py:77
  126.9 0.9 constant_dynamic-slice_fusion.5
  127.9 1.9 bitcast_reduce_fusion.2
  129.8 2.4 %fusion.82 = f32[1,4,384,64]{2,3,1,0:T(8,128)S(1)} fusion(f32[384,384,4]{1,0,2:T(8,128)} %get-tuple-element.151, f32[4,384]{1,0:T(4,128)S(1)} %bitcast.136, f32[1,4,384,64]{2,3,1,0:T(8,128)S(1)} %get-tuple-element.164, f32[4,384]{1,0:T(4,128)S(1)} %get-tuple-element.152, pred[]{:T(512)S(6)} %compare.18, bf16[384,128]{0,1:T(8,128)(2,1)S(1)} %bitcast.134), kind=kOutput, calls=%fused_computation.9.clone.1 | convolution fusion | flops 77561856 | bytes 3207169 | tf_op jit(solution)/shard_map/while/body/eval_jaxpr/kgqs,skd->kgqd/dot_general | solution.py:77
  133.7 1.9 bitcast_reduce_fusion.2
  135.6 2.4 %fusion.82 = f32[1,4,384,64]{2,3,1,0:T(8,128)S(1)} fusion(f32[384,384,4]{1,0,2:T(8,128)} %get-tuple-element.151, f32[4,384]{1,0:T(4,128)S(1)} %bitcast.136, f32[1,4,384,64]{2,3,1,0:T(8,128)S(1)} %get-tuple-element.164, f32[4,384]{1,0:T(4,128)S(1)} %get-tuple-element.152, pred[]{:T(512)S(6)} %compare.18, bf16[384,128]{0,1:T(8,128)(2,1)S(1)} %bitcast.134), kind=kOutput, calls=%fused_computation.9.clone.1 | convolution fusion | flops 77561856 | bytes 3207169 | tf_op jit(solution)/shard_map/while/body/eval_jaxpr/kgqs,skd->kgqd/dot_general | solution.py:77
  138.5 0.9 constant_dynamic-slice_fusion.5
  139.5 1.9 bitcast_reduce_fusion.2
  141.5 2.4 %fusion.82 = f32[1,4,384,64]{2,3,1,0:T(8,128)S(1)} fusion(f32[384,384,4]{1,0,2:T(8,128)} %get-tuple-element.151, f32[4,384]{1,0:T(4,128)S(1)} %bitcast.136, f32[1,4,384,64]{2,3,1,0:T(8,128)S(1)} %get-tuple-element.164, f32[4,384]{1,0:T(4,128)S(1)} %get-tuple-element.152, pred[]{:T(512)S(6)} %compare.18, bf16[384,128]{0,1:T(8,128)(2,1)S(1)} %bitcast.134), kind=kOutput, calls=%fused_computation.9.clone.1 | convolution fusion | flops 77561856 | bytes 3207169 | tf_op jit(solution)/shard_map/while/body/eval_jaxpr/kgqs,skd->kgqd/dot_general | solution.py:77
  145.4 1.9 bitcast_reduce_fusion.2
  147.3 2.4 %fusion.82 = f32[1,4,384,64]{2,3,1,0:T(8,128)S(1)} fusion(f32[384,384,4]{1,0,2:T(8,128)} %get-tuple-element.151, f32[4,384]{1,0:T(4,128)S(1)} %bitcast.136, f32[1,4,384,64]{2,3,1,0:T(8,128)S(1)} %get-tuple-element.164, f32[4,384]{1,0:T(4,128)S(1)} %get-tuple-element.152, pred[]{:T(512)S(6)} %compare.18, bf16[384,128]{0,1:T(8,128)(2,1)S(1)} %bitcast.134), kind=kOutput, calls=%fused_computation.9.clone.1 | convolution fusion | flops 77561856 | bytes 3207169 | tf_op jit(solution)/shard_map/while/body/eval_jaxpr/kgqs,skd->kgqd/dot_general | solution.py:77
  151.2 1.9 bitcast_reduce_fusion.2
  153.1 2.4 %fusion.82 = f32[1,4,384,64]{2,3,1,0:T(8,128)S(1)} fusion(f32[384,384,4]{1,0,2:T(8,128)} %get-tuple-element.151, f32[4,384]{1,0:T(4,128)S(1)} %bitcast.136, f32[1,4,384,64]{2,3,1,0:T(8,128)S(1)} %get-tuple-element.164, f32[4,384]{1,0:T(4,128)S(1)} %get-tuple-element.152, pred[]{:T(512)S(6)} %compare.18, bf16[384,128]{0,1:T(8,128)(2,1)S(1)} %bitcast.134), kind=kOutput, calls=%fused_computation.9.clone.1 | convolution fusion | flops 77561856 | bytes 3207169 | tf_op jit(solution)/shard_map/while/body/eval_jaxpr/kgqs,skd->kgqd/dot_general | solution.py:77
  156.0 3.0 %bitcast_convert_fusion = bf16[384,2048]{1,0:T(8,128)(2,1)} fusion(bf16[4,64,2048]{2,1,0:T(8,128)(2,1)} %bitcast.146, f32[1,4,384,64]{2,3,1,0:T(8,128)S(1)} %get-tuple-element.35, f32[4,384]{1,0:T(4,128)S(1)} %bitcast.142), kind=kOutput, calls=%fused_computation.40 | convolution fusion | flops 403636224 | bytes 3020800 | tf_op jit(solution)/shard_map/kgqd,kgde->qe/dot_general | solution.py:100
  159.0 2.1 slice.56
  161.1 3.8 %all-to-all-start.1 = ((bf16[8,96,512]{2,1,0:T(8,128)(2,1)}), bf16[8,96,512]{2,1,0:T(8,128)(2,1)S(1)}, u32[]{:S(2)}, u32[]{:S(2)}) async-start(bf16[8,96,512]{2,1,0:T(8,128)(2,1)} %bitcast.139), calls=%async_computation.2 | async-start | bytes 1572864 | tf_op jit(solution)/shard_map/all_to_all | solution.py:179
  165.1 39.5 %all-gather.6.cloned.1.call-done = bf16[1536,2048]{1,0:T(8,128)(2,1)} async-done(((bf16[384,2048]{1,0:T(8,128)(2,1)}), bf16[1536,2048]{1,0:T(8,128)(2,1)}) %all-gather.6.cloned.1.call-update) | async-done | bytes 6291472 | tf_op jit(solution)/shard_map/all_gather | solution.py:103
  204.5 5.7 %reduce_sum.90 = bf16[384,2048]{1,0:T(8,128)(2,1)} reduce(bf16[4,384,2048]{2,1,0:T(8,128)(2,1)} %bitcast.135, bf16[]{:T(256)} %constant.129.clone.1), dimensions={0}, to_apply=%region_6.7 | reduce | flops 2359296 | bytes 7864322 | tf_op jit(solution)/shard_map/reduce_sum | solution.py:103
  210.2 1.9 fusion.21
  212.1 1.6 fusion.23
  213.7 2.6 %gather_fusion.1 = bf16[512,512]{1,0:T(8,128)(2,1)} fusion(bf16[768,512]{1,0:T(8,128)(2,1)S(1)} %bitcast.132, s32[1024]{0:T(1024)S(1)} %pad_clamp_fusion), kind=kCustom, calls=%fused_computation.1 | custom fusion | bytes 1050624 | tf_op jit(solution)/shard_map/gather | solution.py:180
  216.3 1.7 reshape.421
  218.0 1.3 multiply_reduce_fusion
  219.3 1.7 add_convert_fusion
  (141 shorter events, 13.0 us)
Async XLA Ops:
  7.2 81.0 %copy-start = (bf16[512,2048]{1,0:T(8,128)(2,1)S(1)}, bf16[512,2048]{1,0:T(8,128)(2,1)}, u32[]{:S(2)}) copy-start(bf16[512,2048]{1,0:T(8,128)(2,1)} %param.35) | copy-start | bytes 6291460
  7.2 8.0 %copy-start.3 = (bf16[256,2048]{1,0:T(8,128)(2,1)S(1)}, bf16[256,2048]{1,0:T(8,128)(2,1)}, u32[]{:S(2)}) copy-start(bf16[256,2048]{1,0:T(8,128)(2,1)} %param.26) | copy-start | bytes 3145732
  7.2 85.3 %all-gather.4.cloned.1.call-start = ((), (), s32[]{:S(2)}) async-start(), calls=%async_computation.3 | async-start | bytes 3932160 | tf_op jit(solution)/shard_map/all_gather | solution.py:156
  16.1 1.0 copy-start.4
  19.8 29.0 %copy-start.10 = (f32[64]{0:T(128)S(1)}, f32[64]{0:T(128)}, u32[]{:S(2)}) copy-start(f32[64]{0:T(128)} %param.23) | copy-start | bytes 772
  19.8 29.5 %copy-start.7 = (bf16[384,256]{1,0:T(8,128)(2,1)S(1)}, bf16[384,256]{1,0:T(8,128)(2,1)}, u32[]{:S(2)}) copy-start(bf16[384,256]{1,0:T(8,128)(2,1)} %param.19) | copy-start | bytes 589828
  20.0 29.9 %copy-start.11 = (f32[64]{0:T(128)S(1)}, f32[64]{0:T(128)}, u32[]{:S(2)}) copy-start(f32[64]{0:T(128)} %param.22) | copy-start | bytes 772
  47.4 111.6 %reduce-scatter.2.cloned.1.call-start = ((), (), s32[]{:S(2)}) async-start(), calls=%async_computation.4 | async-start | bytes 5242880 | tf_op jit(solution)/shard_map/reduce_scatter | solution.py:170
  49.5 1.2 copy-start.5
  92.5 6.3 %copy-start.12 = (bf16[1,2048,1024]{2,1,0:T(8,128)(2,1)S(1)}, bf16[1,2048,1024]{2,1,0:T(8,128)(2,1)}, u32[]{:S(2)}) copy-start(bf16[1,2048,1024]{2,1,0:T(8,128)(2,1)} %param.31) | copy-start | bytes 12582916
  92.5 6.3 %copy-start.14 = (bf16[1,768,2048]{2,1,0:T(8,128)(2,1)S(1)}, bf16[1,768,2048]{2,1,0:T(8,128)(2,1)}, u32[]{:S(2)}) copy-start(bf16[1,768,2048]{2,1,0:T(8,128)(2,1)} %all-gather.4.cloned.1.call-done) | copy-start | bytes 9437188
  98.8 3.6 %copy-start.13 = (bf16[1,1024,2048]{2,1,0:T(8,128)(2,1)S(1)}, bf16[1,1024,2048]{2,1,0:T(8,128)(2,1)}, u32[]{:S(2)}) copy-start(bf16[1,1024,2048]{2,1,0:T(8,128)(2,1)} %param.32) | copy-start | bytes 12582916
  102.4 3.6 %copy-start.6 = (bf16[256,2048]{1,0:T(8,128)(2,1)S(1)}, bf16[256,2048]{1,0:T(8,128)(2,1)}, u32[]{:S(2)}) copy-start(bf16[256,2048]{1,0:T(8,128)(2,1)} %convolution_convert_fusion) | copy-start | bytes 3145732
  108.4 96.1 %all-gather.6.cloned.1.call-start = ((), (), s32[]{:S(2)}) async-start(), calls=%async_computation.5 | async-start | bytes 7864320 | tf_op jit(solution)/shard_map/all_gather | solution.py:103
  111.4 3.1 %copy-start.1 = (f32[384,384,4]{1,0,2:T(8,128)S(1)}, f32[384,384,4]{1,0,2:T(8,128)}, u32[]{:S(2)}) copy-start(f32[384,384,4]{1,0,2:T(8,128)} %get-tuple-element.151) | copy-start | bytes 7077892 | tf_op jit(solution)/shard_map/while
  117.9 2.5 %copy-start.1 = (f32[384,384,4]{1,0,2:T(8,128)S(1)}, f32[384,384,4]{1,0,2:T(8,128)}, u32[]{:S(2)}) copy-start(f32[384,384,4]{1,0,2:T(8,128)} %get-tuple-element.151) | copy-start | bytes 7077892 | tf_op jit(solution)/shard_map/while
  123.8 2.6 %copy-start.1 = (f32[384,384,4]{1,0,2:T(8,128)S(1)}, f32[384,384,4]{1,0,2:T(8,128)}, u32[]{:S(2)}) copy-start(f32[384,384,4]{1,0,2:T(8,128)} %get-tuple-element.151) | copy-start | bytes 7077892 | tf_op jit(solution)/shard_map/while
  129.8 2.4 %copy-start.1 = (f32[384,384,4]{1,0,2:T(8,128)S(1)}, f32[384,384,4]{1,0,2:T(8,128)}, u32[]{:S(2)}) copy-start(f32[384,384,4]{1,0,2:T(8,128)} %get-tuple-element.151) | copy-start | bytes 7077892 | tf_op jit(solution)/shard_map/while
  135.6 2.4 %copy-start.1 = (f32[384,384,4]{1,0,2:T(8,128)S(1)}, f32[384,384,4]{1,0,2:T(8,128)}, u32[]{:S(2)}) copy-start(f32[384,384,4]{1,0,2:T(8,128)} %get-tuple-element.151) | copy-start | bytes 7077892 | tf_op jit(solution)/shard_map/while
  141.4 2.4 %copy-start.1 = (f32[384,384,4]{1,0,2:T(8,128)S(1)}, f32[384,384,4]{1,0,2:T(8,128)}, u32[]{:S(2)}) copy-start(f32[384,384,4]{1,0,2:T(8,128)} %get-tuple-element.151) | copy-start | bytes 7077892 | tf_op jit(solution)/shard_map/while
  147.3 2.4 %copy-start.1 = (f32[384,384,4]{1,0,2:T(8,128)S(1)}, f32[384,384,4]{1,0,2:T(8,128)}, u32[]{:S(2)}) copy-start(f32[384,384,4]{1,0,2:T(8,128)} %get-tuple-element.151) | copy-start | bytes 7077892 | tf_op jit(solution)/shard_map/while
  153.1 2.4 %copy-start.1 = (f32[384,384,4]{1,0,2:T(8,128)S(1)}, f32[384,384,4]{1,0,2:T(8,128)}, u32[]{:S(2)}) copy-start(f32[384,384,4]{1,0,2:T(8,128)} %get-tuple-element.151) | copy-start | bytes 7077892 | tf_op jit(solution)/shard_map/while
  158.9 5.9 %copy-start.9 = (f32[256,2]{0,1:T(2,128)S(1)}, f32[256,2]{0,1:T(2,128)}, u32[]{:S(2)}) copy-start(f32[256,2]{0,1:T(2,128)} %param.28) | copy-start | bytes 6148
  161.1 52.6 %all-to-all-start.1 = ((bf16[8,96,512]{2,1,0:T(8,128)(2,1)}), bf16[8,96,512]{2,1,0:T(8,128)(2,1)S(1)}, u32[]{:S(2)}, u32[]{:S(2)}) async-start(bf16[8,96,512]{2,1,0:T(8,128)(2,1)} %bitcast.139), calls=%async_computation.2 | async-start | bytes 1572864 | tf_op jit(solution)/shard_map/all_to_all | solution.py:179
  204.5 7.6 %copy-start.8 = (f32[2048]{0:T(1024)S(1)}, f32[2048]{0:T(1024)}, u32[]{:S(2)}) copy-start(f32[2048]{0:T(1024)} %param.25) | copy-start | bytes 24580
  210.2 1.9 copy-start.2
Sparse Core Ops, SparseCore 0:
  47.5 27.5 all-gather.3
  108.6 43.3 reduce-scatter.1
  159.1 45.3 all-gather.5
